TPU v7x, 32 devices: a whole 2x2x4 slice. The times are simulated.
32 devices in a mesh: sp: 4 (over y, x), tp: 8 (over z, core).
Axes of the slice: x: 2, y: 2, z: 4, core: 2. Of those that a mesh axis runs over, the one named last changes fastest.
Arguments:
- queries: bfloat16 [3072, 16, 128], P('sp', 'tp'), may hold values from -240 to 240
- key_pairs: bfloat16 [3072, 16, 128], P('sp', 'tp'), may hold values from -11 to 11
- head_values: bfloat16 [3072, 16, 128], P('sp', 'tp'), may hold values from -6 to 6
- lambdas: float32 [16], P('tp'), may hold values from 0.3 to 0.8
- head_gain: float32 [128], replicated, may hold values from 0.1 to 1.9
- out_weight: bfloat16 [2048, 2048], replicated, may hold values from -0.125 to 0.125
- residual: bfloat16 [3072, 2048], P(('sp', 'tp')), may hold values from -6 to 6
- norm_gain: float32 [2048], replicated, may hold values from 0.1 to 1.9
- expert_ids: int32 [3072, 2], P(('sp', 'tp')), may hold values from 0 to 7, all different within a row; in each aligned block of 96 rows (0 to 95, 96 to 191, ...) at most 32 rows name the same one
- route_weights: float32 [3072, 2], P(('sp', 'tp')), may hold values from 0.2 to 1
- gate_weight: bfloat16 [8, 2048, 2048], P('sp', None, 'tp'), may hold values from -0.125 to 0.125
- up_weight: bfloat16 [8, 2048, 2048], P('sp', None, 'tp'), may hold values from -0.125 to 0.125
- down_weight: bfloat16 [8, 2048, 2048], P('sp', 'tp'), may hold values from -0.125 to 0.125
Outputs:
- merged: bfloat16 [3072, 2048], P(('sp', 'tp'))
Inputs may be any that keep to these rules, and one draw needn't show every extreme that they name: `expert_ids`: within the rows of one device each expert is named at most 32 times, and exactly 32 times in some device.
All inputs are finite; a program needn't handle non-finite values.
Results may differ from a plain program's by a relative error of at most 0.019.
Values may be sent and summed in bfloat16 or wider, within the bound.
A program may use at most 128 MiB of HBM per device.

v0:
```python
import math

import jax
import jax.numpy as jnp
from jax import lax
from jax.sharding import PartitionSpec as P


def shards(
    queries,
    key_pairs,
    head_values,
    lambdas,
    head_gain,
    out_weight,
    residual,
    norm_gain,
    expert_ids,
    route_weights,
    gate_weight,
    up_weight,
    down_weight,
):
    tokens_here, heads_here, pair_width = queries.shape
    half_width = pair_width // 2
    value_width = head_values.shape[2]
    score_scale = half_width ** (-0.5)
    query_pos = lax.axis_index("sp") * tokens_here + jnp.arange(tokens_here, dtype=jnp.int32)
    split_queries = queries.reshape(tokens_here, heads_here, 2, half_width)
    start_state = (
        jnp.full((2, heads_here, tokens_here), -1e30, jnp.float32),
        jnp.zeros((2, heads_here, tokens_here), jnp.float32),
        jnp.zeros((2, heads_here, tokens_here, value_width), jnp.float32),
    )
    key_piece = lax.all_gather(key_pairs, "sp", axis=0, tiled=True)
    value_piece = lax.all_gather(head_values, "sp", axis=0, tiled=True)
    span_rows = key_piece.shape[0]
    width_rows = math.gcd(span_rows, 512)

    def block_step(block_index, state):
        running_max, totals, summed = state
        offset = block_index * width_rows
        key_block = lax.dynamic_slice_in_dim(key_piece, offset, width_rows, 0).reshape(
            width_rows, heads_here, 2, half_width
        )
        value_block = lax.dynamic_slice_in_dim(value_piece, offset, width_rows, 0)
        key_pos = offset + jnp.arange(width_rows, dtype=jnp.int32)
        allowed = key_pos[None, :] <= query_pos[:, None]
        scores = (
            jnp.einsum(
                "qhcd,khcd->chqk", split_queries, key_block, preferred_element_type=jnp.float32
            )
            * score_scale
        )
        scores = jnp.where(allowed[None, None], scores, -jnp.inf)
        fresh_max = jnp.maximum(running_max, jnp.max(scores, axis=3))
        decay = jnp.exp(running_max - fresh_max)
        weights = jnp.exp(scores - fresh_max[..., None])
        totals = totals * decay + jnp.sum(weights, axis=3)
        summed = summed * decay[..., None] + jnp.einsum(
            "chqk,khv->chqv",
            weights.astype(jnp.bfloat16),
            value_block,
            preferred_element_type=jnp.float32,
        )
        return (fresh_max, totals, summed)

    def through(state):
        return lax.fori_loop(0, span_rows // width_rows, block_step, state)

    def untouched(state):
        return state

    running_max, totals, summed = lax.cond(
        jnp.int32(0) <= query_pos[-1], through, untouched, start_state
    )
    mixed = (
        summed[0] / totals[0][..., None] - lambdas[:, None, None] * summed[1] / totals[1][..., None]
    )
    normed_heads = (
        mixed * lax.rsqrt(jnp.mean(mixed * mixed, axis=2, keepdims=True) + 1e-06) * head_gain
    )
    attended = (
        jnp.transpose(normed_heads, (1, 0, 2))
        .reshape(tokens_here, heads_here * value_width)
        .astype(jnp.bfloat16)
    )
    rows_here = residual.shape[0]
    regrouped = lax.all_to_all(attended, "tp", split_axis=0, concat_axis=1, tiled=True)
    projected = jnp.dot(regrouped, out_weight, preferred_element_type=jnp.float32)
    updated = (residual.astype(jnp.float32) + projected).astype(jnp.bfloat16)
    widened = updated.astype(jnp.float32)
    normed = (
        widened * lax.rsqrt(jnp.mean(widened * widened, axis=1, keepdims=True) + 1e-06) * norm_gain
    ).astype(jnp.bfloat16)
    route_count = expert_ids.shape[1]
    local_experts = gate_weight.shape[0]
    sp_count = lax.axis_size("sp")
    expert_count = local_experts * sp_count
    capacity = max(2, 4 * rows_here * route_count // (3 * expert_count))
    model_width = normed.shape[1]
    flat_ids = expert_ids.reshape(-1)
    indicator = (flat_ids[:, None] == jnp.arange(expert_count, dtype=jnp.int32)[None, :]).astype(
        jnp.int32
    )
    ranking = jnp.sum(jnp.cumsum(indicator, axis=0) * indicator, axis=1) - 1
    slots = flat_ids * capacity + ranking
    sources = jnp.arange(rows_here * route_count, dtype=jnp.int32) // route_count
    outgoing = (
        jnp.zeros((expert_count * capacity, model_width), jnp.bfloat16)
        .at[slots]
        .set(normed[sources])
    )
    arrived = lax.all_to_all(
        outgoing.reshape(sp_count, local_experts, capacity, model_width),
        "sp",
        split_axis=0,
        concat_axis=0,
        tiled=True,
    )
    piece_rows = lax.all_gather(arrived[None], "tp", axis=0, tiled=True)
    gate_part = jnp.einsum(
        "tsecd,edf->tsecf", piece_rows, gate_weight, preferred_element_type=jnp.float32
    )
    up_part = jnp.einsum(
        "tsecd,edf->tsecf", piece_rows, up_weight, preferred_element_type=jnp.float32
    )
    inner_rows = (jax.nn.silu(gate_part) * up_part).astype(jnp.bfloat16)
    partial_value = jnp.einsum(
        "tsecf,efd->tsecd", inner_rows, down_weight, preferred_element_type=jnp.float32
    )
    reduced = lax.psum_scatter(
        partial_value.astype(jnp.bfloat16), "tp", scatter_dimension=0, tiled=True
    )
    returned = lax.all_to_all(reduced[0], "sp", split_axis=0, concat_axis=0, tiled=True)
    picked = (
        returned.reshape(expert_count * capacity, model_width)[slots]
        .astype(jnp.float32)
        .reshape(rows_here, route_count, model_width)
    )
    moe_sum = jnp.sum(picked * route_weights[:, :, None], axis=1)
    return (updated.astype(jnp.float32) + moe_sum).astype(jnp.bfloat16)


def solution(mesh):
    placed = (
        P("sp", "tp", None),
        P("sp", "tp", None),
        P("sp", "tp", None),
        P("tp"),
        P(),
        P(),
        P(("sp", "tp"), None),
        P(),
        P(("sp", "tp"), None),
        P(("sp", "tp"), None),
        P("sp", None, "tp"),
        P("sp", None, "tp"),
        P("sp", "tp", None),
    )
    return jax.shard_map(
        shards, mesh=mesh, in_specs=placed, out_specs=P(("sp", "tp"), None), check_vma=False
    )
```

profile of v0, /device:TPU:0, one launch (start us, length us, event | category | flops | bytes accessed | tf_op | source)
XLA Modules:
  0.0 527.9 jit_solution(12281369762968562152)
XLA Ops:
  6.5 2.1 copy.39
  8.7 1.9 copy.40
  13.1 29.7 %all-gather.5.cloned.1.call-done = bf16[3072,2,128]{0,2,1:T(8,128)(2,1)} async-done(((bf16[768,2,128]{0,2,1:T(8,128)(2,1)}), bf16[3072,2,128]{0,2,1:T(8,128)(2,1)}) %all-gather.5.cloned.1.call-update) | async-done | bytes 1572880 | tf_op jit(solution)/shard_map/all_gather | solution.py:35
  42.8 32.7 %all-gather.7.cloned.1.call-done = bf16[3072,2,128]{0,2,1:T(8,128)(2,1)} async-done(((bf16[768,2,128]{0,2,1:T(8,128)(2,1)}), bf16[3072,2,128]{0,2,1:T(8,128)(2,1)}) %all-gather.7.cloned.1.call-update) | async-done | bytes 1572880 | tf_op jit(solution)/shard_map/all_gather | solution.py:36
  75.5 83.6 %conditional.1 = (f32[2,2,768]{2,1,0:T(2,128)}, f32[2,2,768,128]{2,3,0,1:T(8,128)}) conditional(s32[]{:T(128)} %bitcast.1, () %tuple.27, (bf16[768,2,128]{2,1,0:T(2,128)(2,1)S(1)}, s32[768]{0:T(1024)S(1)}, bf16[3072,2,128]{0,2,1:T(8,128)(2,1)}, bf16[3072,2,128]{0,2,1:T(8,128)(2,1)}) %tuple.70), branch_computations={%region_0.0_spmd, %region_1.6_spmd} | conditional | flops 618151424 | bytes 26430768 | solution.py:74
  76.0 83.1 %while.17 = (s32[]{:T(128)}, f32[2,2,768]{2,1,0:T(2,128)S(1)}, f32[2,2,768]{2,1,0:T(2,128)}, f32[2,2,768,128]{2,3,0,1:T(8,128)}, s32[768]{0:T(1024)S(1)}, /*inde...) while((s32[]{:T(128)}, f32[2,2,768]{2,1,0:T(2,128)S(1)}, ...), condition=%wide.region_5.5_spmd.clone, body=%wide.region_2.4_spmd.clone.sunk | while | flops 618151424 | bytes 24857784 | solution.py:69
  77.3 3.9 fusion.56
  81.2 4.3 fusion.58
  86.1 2.7 bitcast_add_fusion.2
  90.1 3.9 fusion.56
  94.0 4.3 fusion.58
  98.3 1.3 fusion.59
  99.6 3.3 bitcast_add_fusion.2
  104.2 3.9 fusion.56
  108.0 4.3 fusion.58
  112.3 1.3 fusion.59
  113.7 3.3 bitcast_add_fusion.2
  118.2 3.9 fusion.56
  122.1 4.3 fusion.58
  126.4 1.3 fusion.59
  127.7 3.3 bitcast_add_fusion.2
  132.3 3.9 fusion.56
  136.2 4.3 fusion.58
  140.4 1.3 fusion.59
  141.8 3.3 bitcast_add_fusion.2
  146.3 3.9 fusion.56
  150.2 4.3 fusion.58
  154.5 1.3 fusion.59
  155.8 3.3 bitcast_add_fusion.2
  159.9 1.6 multiply_reduce_fusion.2
  162.1 1.0 convert_element_type.62
  163.1 4.6 all-to-all-start
  168.0 12.2 %all-to-all-done = bf16[8,96,256]{2,1,0:T(8,128)(2,1)S(1)} async-done(((bf16[8,96,256]{2,1,0:T(8,128)(2,1)}), bf16[8,96,256]{2,1,0:T(8,128)(2,1)S(1)}, u32[]{:S(2)}, u32[]{:S(2)}) %all-to-all-start) | async-done | bytes 393248 | tf_op jit(solution)/shard_map/all_to_all | solution.py:89
  180.3 5.0 multiply_reduce_fusion.1
  186.3 4.5 scatter_custom_fusion
  190.9 17.2 %all_to_all.26 = bf16[4,2,32,2048]{3,2,1,0:T(8,128)(2,1)} all-to-all(bf16[4,2,32,2048]{3,2,1,0:T(8,128)(2,1)S(1)} %bitcast.127), channel_id=1, replica_groups=mesh['sp'=4,'tp'=8] {'sp'}, dimensions={0} | all-to-all | bytes 2097152 | tf_op jit(solution)/shard_map/all_to_all | solution.py:114
  208.1 80.3 %all-gather.9.cloned.1.call-done = bf16[32,2,32,2048]{3,2,1,0:T(8,128)(2,1)} async-done(((bf16[4,2,32,2048]{3,2,1,0:T(8,128)(2,1)}), bf16[32,2,32,2048]{3,2,1,0:T(8,128)(2,1)}) %all-gather.9.cloned.1.call-update) | async-done | bytes 8388624 | tf_op jit(solution)/shard_map/all_gather | solution.py:121
  288.4 8.4 %copy.47 = bf16[32,2,32,2048]{3,2,0,1:T(8,128)(2,1)} copy(bf16[32,2,32,2048]{3,2,1,0:T(8,128)(2,1)} %all-gather.9.cloned.1.call-done) | data formatting | bytes 16777216 | tf_op jit(solution)/shard_map/all_gather | solution.py:121
  296.9 7.1 %fusion.17 = f32[2,8,4,32,256]{4,3,2,1,0:T(8,128)} fusion(bf16[8,4,2,32,2048]{4,3,1,0,2:T(8,128)(2,1)} %bitcast.124, bf16[2,2048,256]{2,1,0:T(8,128)(2,1)S(1)} %copy-done.10), kind=kOutput, calls=%fused_computation.30 | convolution fusion | flops 2147483648 | bytes 12582912 | tf_op jit(solution)/shard_map/tsecd,edf->tsecf/dot_general | solution.py:125
  303.9 13.5 %convert_bitcast_fusion = bf16[8,4,2,32,2048]{4,3,1,0,2:T(8,128)(2,1)} fusion(bf16[2,256,2048]{2,1,0:T(8,128)(2,1)S(1)} %copy-done, f32[2,8,4,32,256]{4,3,2,1,0:T(8,128)} %fusion.17, bf16[8,4,2,32,2048]{4,3,1,0,2:T(8,128)(2,1)} %bitcast.125, bf16[2,2048,256]{2,1,0:T(8,128)(2,1)} %param.27), kind=kOutput, calls=%fused_computation.25 | convolution fusion | flops 4302307328 | bytes 23068672 | tf_op jit(solution)/shard_map/tsecf,efd->tsecd/dot_general | solution.py:129
  318.7 173.0 %all-reduce.4.cloned.1.call-done = bf16[8,4,2,32,2048]{4,3,1,0,2:T(8,128)(2,1)} async-done(((bf16[8,4,2,32,2048]{4,3,1,0,2:T(8,128)(2,1)}), bf16[8,4,2,32,2048]{4,3,1,0,2:T(8,128)(2,1)}) %all-reduce.4.cloned.1.call-update) | async-done | bytes 8388624
  491.6 1.9 dynamic-slice_bitcast_fusion
  493.6 1.0 copy.48
  494.6 3.6 all-to-all-start.2
  498.4 13.3 %all-to-all-done.2 = bf16[4,2,32,2048]{3,2,1,0:T(8,128)(2,1)S(1)} async-done(((bf16[4,2,32,2048]{3,2,1,0:T(8,128)(2,1)}), bf16[4,2,32,2048]{3,2,1,0:T(8,128)(2,1)S(1)}, u32[]{:S(2)}, u32[]{:S(2)}) %all-to-all-start.2) | async-done | bytes 1048608 | tf_op jit(solution)/shard_map/all_to_all | solution.py:135
  511.7 2.0 gather_fusion
  513.8 3.0 reshape.182
  516.8 3.7 multiply_reduce_fusion
  (104 shorter events, 15.6 us)
Async XLA Ops:
  6.5 297.4 %copy-start = (bf16[2,256,2048]{2,1,0:T(8,128)(2,1)S(1)}, bf16[2,256,2048]{2,1,0:T(8,128)(2,1)}, u32[]{:S(2)}) copy-start(bf16[2,256,2048]{2,1,0:T(8,128)(2,1)} %param.29) | copy-start | bytes 6291460
  6.5 5.4 %copy-start.6 = (s32[96,2]{0,1:T(2,128)S(1)}, s32[96,2]{0,1:T(2,128)}, u32[]{:S(2)}) copy-start(s32[96,2]{0,1:T(2,128)} %param.25) | copy-start | bytes 2308
  6.5 69.0 %copy-start.3 = (bf16[768,2,128]{2,1,0:T(2,128)(2,1)S(1)}, bf16[768,2,128]{2,1,0:T(2,128)(2,1)}, u32[]{:S(2)}) copy-start(bf16[768,2,128]{2,1,0:T(2,128)(2,1)} %param.17) | copy-start | bytes 1179652
  6.5 36.2 %all-gather.5.cloned.1.call-start = ((), (), s32[]{:S(2)}) async-start(), calls=%async_computation.3 | async-start | bytes 1966080 | tf_op jit(solution)/shard_map/all_gather | solution.py:35
  8.6 66.9 %all-gather.7.cloned.1.call-start = ((), (), s32[]{:S(2)}) async-start(), calls=%async_computation.4 | async-start | bytes 1966080 | tf_op jit(solution)/shard_map/all_gather | solution.py:36
  75.5 84.3 %copy-start.8 = (f32[2]{0:T(128)S(1)}, f32[2]{0:T(128)}, u32[]{:S(2)}) copy-start(f32[2]{0:T(128)} %param.20) | copy-start | bytes 28
  159.1 2.4 copy-start.9
  161.5 18.7 %copy-start.4 = (bf16[96,2048]{1,0:T(8,128)(2,1)S(1)}, bf16[96,2048]{1,0:T(8,128)(2,1)}, u32[]{:S(2)}) copy-start(bf16[96,2048]{1,0:T(8,128)(2,1)} %param.23) | copy-start | bytes 1179652
  163.1 17.1 %all-to-all-start = ((bf16[8,96,256]{2,1,0:T(8,128)(2,1)}), bf16[8,96,256]{2,1,0:T(8,128)(2,1)S(1)}, u32[]{:S(2)}, u32[]{:S(2)}) async-start(bf16[8,96,256]{2,1,0:T(8,128)(2,1)} %convert_element_type.62), calls=%async_computation | async-start | bytes 786432 | tf_op jit(solution)/shard_map/all_to_all | solution.py:89
  167.7 120.8 %all-gather.9.cloned.1.call-start = ((), (), s32[]{:S(2)}) async-start(), calls=%async_computation.5 | async-start | bytes 9437184 | tf_op jit(solution)/shard_map/all_gather | solution.py:121
  180.2 5.9 %copy-start.5 = (f32[2048]{0:T(1024)S(1)}, f32[2048]{0:T(1024)}, u32[]{:S(2)}) copy-start(f32[2048]{0:T(1024)} %param.24) | copy-start | bytes 24580
  185.3 0.9 copy-start.1
  208.1 283.5 %all-reduce.4.cloned.1.call-start = ((), (), s32[]{:S(2)}) async-start(), calls=%async_computation.6 | async-start | bytes 16777216
  288.4 8.4 %copy-start.10 = (bf16[2,2048,256]{2,1,0:T(8,128)(2,1)S(1)}, bf16[2,2048,256]{2,1,0:T(8,128)(2,1)}, u32[]{:S(2)}) copy-start(bf16[2,2048,256]{2,1,0:T(8,128)(2,1)} %param.28) | copy-start | bytes 6291460
  317.4 0.7 copy-start.11
  493.6 4.7 copy-start.7
  494.6 17.1 %all-to-all-start.2 = ((bf16[4,2,32,2048]{3,2,1,0:T(8,128)(2,1)}), bf16[4,2,32,2048]{3,2,1,0:T(8,128)(2,1)S(1)}, u32[]{:S(2)}, u32[]{:S(2)}) async-start(bf16[4,2,32,2048]{3,2,1,0:T(8,128)(2,1)} %copy.48), calls=%async_computation.2 | async-start | bytes 2097152 | tf_op jit(solution)/shard_map/all_to_all | solution.py:135
  513.8 6.8 %copy-start.2 = (f32[96,2048]{1,0:T(8,128)S(1)}, f32[96,2048]{1,0:T(8,128)}, u32[]{:S(2)}) copy-start(f32[96,2048]{1,0:T(8,128)} %copy-done.1) | copy-start | bytes 2359300
Sparse Core Ops, SparseCore 0:
  9.2 33.5 all-gather.4
  44.6 30.8 all-gather.6
  208.2 80.1 all-gather.8
  317.6 174.0 all-reduce.3
where the time goes:
time: 529 us; the launch traced here: 528 us
  waiting for transfers between devices  341 us (64%)
  matrix products  67.9 us (13%)
  other arithmetic  41.9 us (8%)
  local copies, waits for them, and re-layouts  37.1 us (7%)
  blocking collectives  17.2 us (3%)
  between operations  14 us (3%)
  starting transfers between devices  8.38 us (2%)
    unnamed x5, waiting for transfers between devices  173 us
    all_gather x1, waiting for transfers between devices, shards(): piece_rows = lax.all_gather(arrived[None], 'tp', axis=0, tiled=True)  80.3 us
    all_gather x1, waiting for transfers between devices, shards(): value_piece = lax.all_gather(head_values, 'sp', axis=0, tiled=True)  32.7 us
    all_gather x1, waiting for transfers between devices, shards(): key_piece = lax.all_gather(key_pairs, 'sp', axis=0, tiled=True)  29.7 us
    convert_element_type x6, other arithmetic, block_step(): weights.astype(jnp.bfloat16)  25.6 us
    dot_general x6, matrix products, block_step(): jnp.einsum('qhcd,khcd->chqk', split_queries, key_block, preferred_element...  23.2 us
    dot_general x6, matrix products, block_step(): jnp.einsum('chqk,khv->chqv', weights.astype(jnp.bfloat16), value_block, p...  19.2 us
    all_to_all x1, blocking collectives, shards(): lax.all_to_all(outgoing.reshape(sp_count, local_experts, capacity, model_...  17.2 us
  transfers between devices with their start and end apart: 6, of which 6 were waited for; matrix products, arithmetic and copies ran while one was open for 1% of the time, Pallas kernels for 0%

commit v1 on v0

v1 whole, which is shorter than its diff:
```python
import functools
import math

import jax
import jax.numpy as jnp
from jax import lax
from jax.experimental import pallas as pl
from jax.experimental.pallas import tpu as pltpu
from jax.sharding import PartitionSpec as P

MESH = pl.DeviceIdType.MESH
LOG2E = 1.4426950408889634
CORES = 2
VMEM_BYTES = 67043328


def attend_kernel(
    n_sp,
    n_tp,
    scale,
    lam_ref,
    q_ref,
    kv_ref,
    gain_ref,
    meta_ref,
    out_ref,
    zmeta_ref,
    kvbuf,
    acc,
    top,
    tot,
    att,
    kv_send,
    kv_recv,
    at_send,
    at_recv,
    me_send,
    me_recv,
    own_sem,
):
    heads, tiles, wide, _ = q_ref.shape
    tile = wide // 2
    rows = out_ref.shape[1]
    n_z = n_tp // CORES
    c = lax.axis_index("sp")
    t = lax.axis_index("tp")
    barrier = pltpu.get_barrier_semaphore()
    for d in range(1, n_sp):
        pl.semaphore_signal(barrier, inc=1, device_id=((c + d) % n_sp, t), device_id_type=MESH)
    for d in range(1, n_tp):
        pl.semaphore_signal(barrier, inc=1, device_id=(c, (t + d) % n_tp), device_id_type=MESH)
    pl.semaphore_wait(barrier, n_sp + n_tp - 2)

    def kv_copy(d, h):
        return pltpu.make_async_remote_copy(
            src_ref=kv_ref.at[h],
            dst_ref=kvbuf.at[d - 1, h],
            send_sem=kv_send.at[d - 1, h],
            recv_sem=kv_recv.at[d - 1, h],
            device_id=((c + d) % n_sp, t),
            device_id_type=MESH,
        )

    def meta_copy(d):
        return pltpu.make_async_remote_copy(
            src_ref=meta_ref,
            dst_ref=zmeta_ref.at[d],
            send_sem=me_send.at[d],
            recv_sem=me_recv.at[d],
            device_id=(c, (t + CORES * d) % n_tp),
            device_id_type=MESH,
        )

    for d in range(1, n_sp):
        @pl.when(c + d < n_sp)
        def _():
            for h in range(heads):
                kv_copy(d, h).start()

    for d in range(1, n_z):
        meta_copy(d).start()
    zmeta_ref[0] = meta_ref[...]

    factor = scale * LOG2E

    def scores_of(h, i, keys):
        return (
            lax.dot_general(
                q_ref[h, i], keys, (((1,), (1,)), ((), ())), preferred_element_type=jnp.float32
            )
            * factor
        )

    for i in range(tiles):
        extent = (i + 1) * tile
        for h in range(heads):
            s = scores_of(h, i, kv_ref[h, 0, :extent])
            row = lax.rem(lax.broadcasted_iota(jnp.int32, (wide, extent), 0), tile) + i * tile
            col = lax.broadcasted_iota(jnp.int32, (wide, extent), 1)
            s = jnp.where(col <= row, s, -jnp.inf)
            high = jnp.max(s, axis=1, keepdims=True)
            p = jnp.exp2(s - high)
            top[h, i] = high
            tot[h, i] = jnp.sum(p, axis=1, keepdims=True)
            acc[h, i] = jnp.dot(
                p.astype(jnp.bfloat16), kv_ref[h, 1, :extent], preferred_element_type=jnp.float32
            )

    def span_step(step, carry):
        for h in range(heads):
            kv_copy(step, h).wait_recv()

        def tile_step(i, inner):
            for h in range(heads):
                s = scores_of(h, i, kvbuf[step - 1, h, 0])
                before = top[h, i]
                high = jnp.maximum(before, jnp.max(s, axis=1, keepdims=True))
                p = jnp.exp2(s - high)
                decay = jnp.exp2(before - high)
                top[h, i] = high
                tot[h, i] = tot[h, i] * decay + jnp.sum(p, axis=1, keepdims=True)
                acc[h, i] = acc[h, i] * decay + jnp.dot(
                    p.astype(jnp.bfloat16),
                    kvbuf[step - 1, h, 1],
                    preferred_element_type=jnp.float32,
                )
            return inner

        return lax.fori_loop(0, tiles, tile_step, carry)

    lax.fori_loop(1, c + 1, span_step, 0)

    for h in range(heads):
        width = acc.shape[3]
        for i in range(tiles):
            both = acc[h, i] / tot[h, i]
            mixed = both[:tile] - lam_ref[h] * both[tile:]
            mean = jnp.mean(mixed * mixed, axis=1, keepdims=True)
            normed = mixed * lax.rsqrt(mean + 1e-06) * gain_ref[...]
            att[i * tile : (i + 1) * tile, h * width : (h + 1) * width] = normed.astype(att.dtype)

    def att_copy(d):
        to = (t + d) % n_tp
        return pltpu.make_async_remote_copy(
            src_ref=att.at[pl.ds(pl.multiple_of(to * rows, rows), rows)],
            dst_ref=out_ref.at[t],
            send_sem=at_send.at[d],
            recv_sem=at_recv.at[d],
            device_id=(c, to),
            device_id_type=MESH,
        )

    for d in range(1, n_tp):
        att_copy(d).start()
    own = pltpu.make_async_copy(
        att.at[pl.ds(pl.multiple_of(t * rows, rows), rows)], out_ref.at[t], own_sem
    )
    own.start()
    own.wait()
    for d in range(1, n_tp):
        att_copy(d).wait()
    for d in range(1, n_z):
        meta_copy(d).wait()
    for d in range(1, n_sp):
        @pl.when(c + d < n_sp)
        def _():
            for h in range(heads):
                kv_copy(d, h).wait_send()


def attend(queries, key_pairs, head_values, lambdas, head_gain, meta, rows, n_sp, n_tp):
    tokens, heads, pair = queries.shape
    width = head_values.shape[2]
    half = pair // 2
    tile = math.gcd(tokens, 256)
    tiles = tokens // tile
    first = (jnp.arange(pair) < half)[None, :]
    q = jnp.transpose(queries, (1, 0, 2)).reshape(heads, tiles, 1, tile, pair)
    sides = jnp.stack([first, ~first])
    q = jnp.where(sides, q, jnp.zeros((), q.dtype)).reshape(heads, tiles, 2 * tile, pair)
    kv = jnp.transpose(jnp.stack([key_pairs, head_values]), (2, 0, 1, 3))
    dma = pltpu.SemaphoreType.DMA
    vmem = pl.BlockSpec(memory_space=pltpu.VMEM)
    n_z = n_tp // CORES
    return pl.pallas_call(
        functools.partial(attend_kernel, n_sp, n_tp, half ** (-0.5)),
        out_shape=(
            jax.ShapeDtypeStruct((n_tp, rows, heads * width), jnp.bfloat16),
            jax.ShapeDtypeStruct((n_z,) + meta.shape, meta.dtype),
        ),
        in_specs=[pl.BlockSpec(memory_space=pltpu.SMEM)] + [vmem] * 4,
        out_specs=(vmem, vmem),
        scratch_shapes=[
            pltpu.VMEM((n_sp - 1,) + kv.shape, kv.dtype),
            pltpu.VMEM((heads, tiles, 2 * tile, width), jnp.float32),
            pltpu.VMEM((heads, tiles, 2 * tile, 1), jnp.float32),
            pltpu.VMEM((heads, tiles, 2 * tile, 1), jnp.float32),
            pltpu.VMEM((tokens, heads * width), jnp.bfloat16),
            dma((n_sp - 1, heads)),
            dma((n_sp - 1, heads)),
            dma((n_tp,)),
            dma((n_tp,)),
            dma((n_z,)),
            dma((n_z,)),
            dma,
        ],
        compiler_params=pltpu.CompilerParams(
            collective_id=0, has_side_effects=True, vmem_limit_bytes=48 * 1024 * 1024
        ),
        name="attend",
    )(lambdas, q, kv, head_gain.reshape(1, -1), meta)


def experts_kernel(
    n_sp,
    n_z,
    x_ref,
    meta_ref,
    base_ref,
    gate_hbm,
    up_hbm,
    down_hbm,
    out_ref,
    gate,
    up,
    down,
    zrows,
    pack,
    arrived,
    psend,
    own,
    precv,
    ret,
    zsend,
    zret,
    w_sem,
    zs_send,
    zs_recv,
    ps_send,
    ps_recv,
    fw_send,
    fw_recv,
    pp_send,
    pp_recv,
    rt_send,
    rt_recv,
    zr_send,
    zr_recv,
):
    rows, model = x_ref.shape
    local, cap = pack.shape[2], pack.shape[3]
    slots = n_sp * local * cap
    c = lax.axis_index("sp")
    t = lax.axis_index("tp")
    n_tp = n_z * CORES
    core = t % CORES
    partner = (c, t + 1 - 2 * core)
    loads = [
        pltpu.make_async_copy(a, b, w_sem.at[i])
        for i, (a, b) in enumerate(((gate_hbm, gate), (up_hbm, up), (down_hbm, down)))
    ]
    for load in loads:
        load.start()

    def column(d):
        return ((c + d) % n_sp, t)

    def layer(d):
        return (c, (t + CORES * d) % n_tp)

    barrier = pltpu.get_barrier_semaphore()
    for d in range(1, n_sp):
        pl.semaphore_signal(barrier, inc=1, device_id=column(d), device_id_type=MESH)
    for d in range(1, n_z):
        pl.semaphore_signal(barrier, inc=1, device_id=layer(d), device_id_type=MESH)
    pl.semaphore_signal(barrier, inc=1, device_id=partner, device_id_type=MESH)
    pl.semaphore_wait(barrier, n_sp + n_z - 1)

    def remote(src, dst, send, recv, target):
        return pltpu.make_async_remote_copy(
            src_ref=src,
            dst_ref=dst,
            send_sem=send,
            recv_sem=recv,
            device_id=target,
            device_id_type=MESH,
        )

    def z_copy(d):
        return remote(x_ref, zrows.at[d - 1], zs_send.at[d], zs_recv.at[d], layer(d))

    def pack_copy(d, s):
        return remote(
            pack.at[d - 1, s], arrived.at[0, d, s], ps_send.at[d, s], ps_recv.at[d, s], column(d)
        )

    def share_copy(d, s):
        return remote(
            arrived.at[0, d, s], arrived.at[1, d, s], fw_send.at[d, s], fw_recv.at[d, s], partner
        )

    def pair_copy(d):
        return remote(psend.at[d], precv.at[d], pp_send.at[d], pp_recv.at[d], partner)

    def back_copy(d):
        return remote(own.at[d], ret.at[d], rt_send.at[d], rt_recv.at[d], column(n_sp - d))

    def z_back(d):
        return remote(
            zsend.at[d], zret.at[d], zr_send.at[d], zr_recv.at[d], layer(n_z - d)
        )

    for d in range(1, n_z):
        z_copy(d).start()

    def route_hits(s, r):
        target = lax.broadcasted_iota(jnp.int32, (slots, rows), 0).astype(jnp.float32)
        return target == meta_ref[s, r : r + 1, :rows]

    for s in range(n_z):
        if s:
            z_copy(s).wait_recv()
        hits = route_hits(s, 0) | route_hits(s, 1)
        pick = jnp.where(hits, 1.0, 0.0).astype(jnp.bfloat16)
        source = x_ref[...] if s == 0 else zrows[s - 1]
        packed = (
            jnp.dot(pick, source, preferred_element_type=jnp.float32)
            .astype(jnp.bfloat16)
            .reshape(n_sp, local, cap, model)
        )
        for d in range(1, n_sp):
            pack[d - 1, s] = packed[d]
            pack_copy(d, s).start()
        arrived[0, 0, s] = packed[0]
        share_copy(0, s).start()

    for load in loads:
        load.wait()

    def reduce_pair(d):
        pair_copy(d).wait_recv()
        total = own[d].astype(jnp.float32) + precv[d].astype(jnp.float32)
        total = total.astype(jnp.bfloat16)
        if d == 0:
            ret[0] = total
        else:
            own[d] = total
            back_copy(d).start()

    for d in range(n_sp):
        if d:
            for s in range(n_z):
                pack_copy(d, s).wait_recv()
                share_copy(d, s).start()
        for s in range(n_z):
            share_copy(d, s).wait_recv()

        def expert_step(e, carry):
            x = arrived[:, d, :, e].reshape(2 * n_z * cap, model)
            gated = jnp.dot(x, gate[e], preferred_element_type=jnp.float32)
            lifted = jnp.dot(x, up[e], preferred_element_type=jnp.float32)
            inner = (gated / (1.0 + jnp.exp(-gated)) * lifted).astype(jnp.bfloat16)
            y = jnp.dot(inner, down[e], preferred_element_type=jnp.float32)
            y = y.astype(jnp.bfloat16).reshape(2, n_z, cap, model)
            own[d, :, e] = y[0]
            psend[d, :, e] = y[1]
            return carry

        lax.fori_loop(0, local, expert_step, 0)
        pair_copy(d).start()
        if d:
            reduce_pair(d - 1)
    reduce_pair(n_sp - 1)
    for d in range(1, n_sp):
        back_copy(d).wait_recv()

    for s in list(range(1, n_z)) + [0]:
        mixing = jnp.where(route_hits(s, 0), meta_ref[s, 2:3, :rows], 0.0) + jnp.where(
            route_hits(s, 1), meta_ref[s, 3:4, :rows], 0.0
        )
        high = mixing.astype(jnp.bfloat16)
        low = (mixing - high.astype(jnp.float32)).astype(jnp.bfloat16)
        back = ret[:, s].reshape(slots, model)
        numbers = (((0,), (0,)), ((), ()))
        merged = lax.dot_general(
            high, back, numbers, preferred_element_type=jnp.float32
        ) + lax.dot_general(low, back, numbers, preferred_element_type=jnp.float32)
        if s:
            zsend[s] = merged.astype(jnp.bfloat16)
            z_back(s).start()
    for s in range(1, n_z):
        z_back(s).wait_recv()
        merged = merged + zret[s].astype(jnp.float32)
    out_ref[...] = (base_ref[...].astype(jnp.float32) + merged).astype(jnp.bfloat16)

    for d in range(1, n_z):
        z_copy(d).wait_send()
        z_back(d).wait_send()
    for d in range(n_sp):
        for s in range(n_z):
            if d:
                pack_copy(d, s).wait_send()
            share_copy(d, s).wait_send()
        pair_copy(d).wait_send()
        if d:
            back_copy(d).wait_send()


def experts(normed, zmeta, updated, gate_weight, up_weight, down_weight, n_sp, n_z, cap):
    rows, model = normed.shape
    local = gate_weight.shape[0]
    dma = pltpu.SemaphoreType.DMA
    vmem = pl.BlockSpec(memory_space=pltpu.VMEM)
    hbm = pl.BlockSpec(memory_space=pl.ANY)
    block = (n_z, local, cap, model)

    def buffer(*shape):
        return pltpu.VMEM(shape, jnp.bfloat16)

    return pl.pallas_call(
        functools.partial(experts_kernel, n_sp, n_z),
        out_shape=jax.ShapeDtypeStruct((rows, model), jnp.bfloat16),
        in_specs=[vmem] * 3 + [hbm] * 3,
        out_specs=vmem,
        scratch_shapes=[
            buffer(*gate_weight.shape),
            buffer(*up_weight.shape),
            buffer(*down_weight.shape),
            buffer(n_z - 1, rows, model),
            buffer(n_sp - 1, *block),
            buffer(2, n_sp, *block),
            buffer(n_sp, *block),
            buffer(n_sp, *block),
            buffer(n_sp, *block),
            buffer(n_sp, *block),
            buffer(n_z, rows, model),
            buffer(n_z, rows, model),
            dma((3,)),
            dma((n_z,)),
            dma((n_z,)),
            dma((n_sp, n_z)),
            dma((n_sp, n_z)),
            dma((n_sp, n_z)),
            dma((n_sp, n_z)),
            dma((n_sp,)),
            dma((n_sp,)),
            dma((n_sp,)),
            dma((n_sp,)),
            dma((n_z,)),
            dma((n_z,)),
        ],
        compiler_params=pltpu.CompilerParams(
            collective_id=1, has_side_effects=True, vmem_limit_bytes=VMEM_BYTES
        ),
        name="experts",
    )(normed, zmeta, updated, gate_weight, up_weight, down_weight)


def shards(
    queries,
    key_pairs,
    head_values,
    lambdas,
    head_gain,
    out_weight,
    residual,
    norm_gain,
    expert_ids,
    route_weights,
    gate_weight,
    up_weight,
    down_weight,
):
    tokens_here, heads_here, pair_width = queries.shape
    value_width = head_values.shape[2]
    rows_here = residual.shape[0]
    sp_count = lax.axis_size("sp")
    tp_count = lax.axis_size("tp")
    z_count = tp_count // CORES
    route_count = expert_ids.shape[1]
    local_experts = gate_weight.shape[0]
    expert_count = local_experts * sp_count
    capacity = max(2, 4 * rows_here * route_count // (3 * expert_count))
    flat_ids = expert_ids.reshape(-1)
    indicator = (flat_ids[:, None] == jnp.arange(expert_count, dtype=jnp.int32)[None, :]).astype(
        jnp.int32
    )
    ranking = jnp.sum(jnp.cumsum(indicator, axis=0) * indicator, axis=1) - 1
    turned = (flat_ids - lax.axis_index("sp") * local_experts) % expert_count
    near_slots = (turned * capacity + ranking).reshape(rows_here, route_count)
    slots = flat_ids * capacity + ranking
    meta = jnp.concatenate([near_slots.astype(jnp.float32), route_weights], axis=1).T
    meta = jnp.pad(meta, ((0, 8 - 2 * route_count), (0, -rows_here % 128)), constant_values=-1.0)
    gathered, zmeta = attend(
        queries, key_pairs, head_values, lambdas, head_gain, meta, rows_here, sp_count, tp_count
    )
    regrouped = jnp.transpose(gathered, (1, 0, 2)).reshape(rows_here, -1)
    projected = jnp.dot(regrouped, out_weight, preferred_element_type=jnp.float32)
    updated = (residual.astype(jnp.float32) + projected).astype(jnp.bfloat16)
    widened = updated.astype(jnp.float32)
    normed = (
        widened * lax.rsqrt(jnp.mean(widened * widened, axis=1, keepdims=True) + 1e-06) * norm_gain
    ).astype(jnp.bfloat16)
    model_width = normed.shape[1]
    block_bytes = z_count * local_experts * capacity * model_width * 2
    if capacity % 16 == 0 and rows_here <= 128 and route_count == 2 and (
        (7 * sp_count - 1) * block_bytes <= 3 * VMEM_BYTES // 5
    ):
        return experts(
            normed, zmeta, updated, gate_weight, up_weight, down_weight, sp_count, z_count, capacity
        )
    sources = jnp.arange(rows_here * route_count, dtype=jnp.int32) // route_count
    outgoing = (
        jnp.zeros((expert_count * capacity, model_width), jnp.bfloat16)
        .at[slots]
        .set(normed[sources])
    )
    arrived = lax.all_to_all(
        outgoing.reshape(sp_count, local_experts, capacity, model_width),
        "sp",
        split_axis=0,
        concat_axis=0,
        tiled=True,
    )
    piece_rows = lax.all_gather(arrived[None], "tp", axis=0, tiled=True)
    gate_part = jnp.einsum(
        "tsecd,edf->tsecf", piece_rows, gate_weight, preferred_element_type=jnp.float32
    )
    up_part = jnp.einsum(
        "tsecd,edf->tsecf", piece_rows, up_weight, preferred_element_type=jnp.float32
    )
    inner_rows = (jax.nn.silu(gate_part) * up_part).astype(jnp.bfloat16)
    partial_value = jnp.einsum(
        "tsecf,efd->tsecd", inner_rows, down_weight, preferred_element_type=jnp.float32
    )
    reduced = lax.psum_scatter(
        partial_value.astype(jnp.bfloat16), "tp", scatter_dimension=0, tiled=True
    )
    returned = lax.all_to_all(reduced[0], "sp", split_axis=0, concat_axis=0, tiled=True)
    picked = (
        returned.reshape(expert_count * capacity, model_width)[slots]
        .astype(jnp.float32)
        .reshape(rows_here, route_count, model_width)
    )
    moe_sum = jnp.sum(picked * route_weights[:, :, None], axis=1)
    return (updated.astype(jnp.float32) + moe_sum).astype(jnp.bfloat16)


def solution(mesh):
    placed = (
        P("sp", "tp", None),
        P("sp", "tp", None),
        P("sp", "tp", None),
        P("tp"),
        P(),
        P(),
        P(("sp", "tp"), None),
        P(),
        P(("sp", "tp"), None),
        P(("sp", "tp"), None),
        P("sp", None, "tp"),
        P("sp", None, "tp"),
        P("sp", "tp", None),
    )
    return jax.shard_map(
        shards, mesh=mesh, in_specs=placed, out_specs=P(("sp", "tp"), None), check_vma=False
    )
```

time: 529 us -> 228 us (0.43)
  waiting for transfers between devices: 341 us -> 0 us
  Pallas kernels: 0 us -> 212 us
  matrix products: 67.9 us -> 5.01 us
  other arithmetic: 41.9 us -> 3.21 us
  local copies, waits for them, and re-layouts: 37.1 us -> 7.46 us
  blocking collectives: 17.2 us -> 0 us
  between operations: 14 us -> 0.15 us
  starting transfers between devices: 8.38 us -> 0 us
    pallas_call x0 -> x2, Pallas kernels: none -> 212 us  [the longest x1 171 us: experts(): pl.pallas_call(functools.partial(experts_kernel, n_sp, n_z), out_shape=ja...]
    unnamed x5 -> x0, waiting for transfers between devices: 173 us -> none
    all_gather x3 -> x0, waiting for transfers between devices: 143 us -> none  [the longest x1 80.3 us: shards(): piece_rows = lax.all_gather(arrived[None], 'tp', axis=0, tiled=True)]
    dot_general x14 -> x0, matrix products: 62.9 us -> none  [the longest x6 23.2 us: block_step(): jnp.einsum('qhcd,khcd->chqk', split_queries, key_block, preferred_element...]
    convert_element_type x8 -> x1, other arithmetic: 26.5 us -> 0.71 us  [shards(): near_slots.astype(jnp.float32)]
    all_to_all x2 -> x0, waiting for transfers between devices: 25.5 us -> none  [the longest x1 13.3 us: shards(): lax.all_to_all(reduced[0], 'sp', split_axis=0, concat_axis=0, tiled=True)]
    all_to_all x1 -> x0, blocking collectives: 17.2 us -> none  [shards(): lax.all_to_all(outgoing.reshape(sp_count, local_experts, capacity, model_...]
    all_gather x1 -> x0, local copies, waits for them, and re-layouts: 8.42 us -> none  [shards(): piece_rows = lax.all_gather(arrived[None], 'tp', axis=0, tiled=True)]
  transfers between devices with their start and end apart: 6 -> 0, of which waited for: 6 -> 0; matrix products, arithmetic and copies ran while one was open for 1% -> 0% of each run, Pallas kernels for 0% -> 0%
where the time goes in v1:
time: 228 us
  Pallas kernels  212 us (93%)
  local copies, waits for them, and re-layouts  7.46 us (3%)
  matrix products  5.01 us (2%)
  other arithmetic  3.21 us (1%)
    pallas_call x1, Pallas kernels, experts(): pl.pallas_call(functools.partial(experts_kernel, n_sp, n_z), out_shape=ja...  171 us
    pallas_call x1, Pallas kernels, attend(): pl.pallas_call(functools.partial(attend_kernel, n_sp, n_tp, half ** (-0.5...  40.2 us
    dot_general x1, matrix products, shards(): jnp.dot(regrouped, out_weight, preferred_element_type=jnp.float32)  5.01 us
    unnamed x12, local copies, waits for them, and re-layouts  4.58 us

profile of v1, /device:TPU:0, one launch (start us, length us, event | category | flops | bytes accessed | tf_op | source)
XLA Modules:
  0.0 227.6 jit_solution(6884405414935572717)
XLA Ops:
  0.0 0.8 copy.20
  0.8 0.1 eq.24
  0.9 0.6 reduce-window.6
  1.5 0.2 slice_reduce_fusion
  1.8 0.1 add_bitcast_fusion
  1.9 0.1 sub.16
  2.0 0.1 copy.21
  2.1 0.7 fusion.8
  2.8 0.7 maximum_bitcast_fusion.1
  3.5 1.2 copy_bitcast_fusion
  4.7 0.1 maximum_bitcast_fusion.kv_ref
  4.9 1.1 copy.17
  5.9 0.1 bitcast_select_fusion.q_ref
  6.0 0.0 copy-start.1
  6.0 0.6 copy-done.1
  6.7 0.0 copy-start.2
  6.7 0.7 copy-done.2
  7.3 40.2 %attend.1 = (bf16[8,96,256]{2,1,0:T(8,128)(2,1)S(1)}, f32[4,8,128]{2,1,0:T(8,128)S(1)}) custom-call(f32[2]{0:T(128)S(1)} %copy-done.1, bf16[2,3,512,128]{3,2,1,0:T(8,128)(2,1)S(1)} %bitcast_select_fusion.q_ref, bf16[2,2,768,128]{3,2,1,0:T(8,128)(2,1)S(1)} %maximum_bitcast_fusion.kv_ref, f32[1,128]{1,0:T(1,128)S(1)} %bitcast.29, f32[8,128]{1,0:T(8,128)S(1)} %pad.9.meta_ref), custom_call_target="tpu_custom_call" | custom-call | tf_op jit(solution)/shard_map/attend/pallas_call | solution.py:185
  47.6 0.0 copy-start
  47.6 0.0 copy-start.4
  47.6 5.0 %fusion.1 = (f32[96]{0:T(128)S(1)}, bf16[96,2048]{1,0:T(8,128)(2,1)S(1)}) fusion(bf16[96,2048]{1,0:T(8,128)(2,1)S(1)} %bitcast.30, bf16[2048,2048]{1,0:T(8,128)(2,1)} %param.18, bf16[96,2048]{1,0:T(8,128)(2,1)} %param.19), kind=kOutput, calls=%fused_computation.4 | convolution fusion | flops 806485888 | bytes 9568640 | tf_op jit(solution)/shard_map/dot_general | solution.py:498
  52.6 0.0 copy-done
  52.7 0.0 copy-start.3
  52.7 0.7 copy-done.3
  53.4 0.0 copy-done.4
  53.4 0.9 fusion.3.x_ref
  54.3 171.5 %experts.1 = bf16[96,2048]{1,0:T(8,128)(2,1)} custom-call(bf16[96,2048]{1,0:T(8,128)(2,1)} %fusion.3.x_ref, f32[4,8,128]{2,1,0:T(8,128)} %copy-done, bf16[96,2048]{1,0:T(8,128)(2,1)} %copy-done.3, bf16[2,2048,256]{2,1,0:T(8,128)(2,1)} %gate_hbm.1, bf16[2,2048,256]{2,1,0:T(8,128)(2,1)} %up_hbm.1, bf16[2,256,2048]{2,1,0:T(8,128)(2,1)} %down_hbm.1), custom_call_target="tpu_custom_call" | custom-call | tf_op jit(solution)/shard_map/experts/pallas_call | solution.py:420
  225.8 1.8 copy.27
  (12 shorter events, 0.2 us)
Async XLA Ops:
  6.0 0.7 copy-start.1
  6.7 0.7 copy-start.2
  47.6 5.1 %copy-start = (f32[4,8,128]{2,1,0:T(8,128)}, f32[4,8,128]{2,1,0:T(8,128)S(1)}, u32[]{:S(2)}) copy-start(f32[4,8,128]{2,1,0:T(8,128)S(1)} %get-tuple-element.8.meta_ref) | copy-start | bytes 49156
  47.6 5.8 %copy-start.4 = (f32[2048]{0:T(1024)S(1)}, f32[2048]{0:T(1024)}, u32[]{:S(2)}) copy-start(f32[2048]{0:T(1024)} %param.20) | copy-start | bytes 24580
  52.7 0.7 copy-start.3

commit v2 on v1

--- a/solution.py
+++ b/solution.py
@@ -23,8 +23,14 @@
     kv_ref,
     gain_ref,
     meta_ref,
-    out_ref,
+    base_ref,
+    norm_ref,
+    w_hbm,
+    updated_ref,
+    normed_ref,
     zmeta_ref,
+    weight,
+    gathered,
     kvbuf,
     acc,
     top,
@@ -37,13 +43,16 @@
     me_send,
     me_recv,
     own_sem,
+    w_sem,
 ):
     heads, tiles, wide, _ = q_ref.shape
     tile = wide // 2
-    rows = out_ref.shape[1]
+    rows = base_ref.shape[0]
     n_z = n_tp // CORES
     c = lax.axis_index("sp")
     t = lax.axis_index("tp")
+    load = pltpu.make_async_copy(w_hbm, weight, w_sem)
+    load.start()
     barrier = pltpu.get_barrier_semaphore()
     for d in range(1, n_sp):
         pl.semaphore_signal(barrier, inc=1, device_id=((c + d) % n_sp, t), device_id_type=MESH)
@@ -143,7 +152,7 @@
         to = (t + d) % n_tp
         return pltpu.make_async_remote_copy(
             src_ref=att.at[pl.ds(pl.multiple_of(to * rows, rows), rows)],
-            dst_ref=out_ref.at[t],
+            dst_ref=gathered.at[t],
             send_sem=at_send.at[d],
             recv_sem=at_recv.at[d],
             device_id=(c, to),
@@ -153,12 +162,29 @@
     for d in range(1, n_tp):
         att_copy(d).start()
     own = pltpu.make_async_copy(
-        att.at[pl.ds(pl.multiple_of(t * rows, rows), rows)], out_ref.at[t], own_sem
+        att.at[pl.ds(pl.multiple_of(t * rows, rows), rows)], gathered.at[t], own_sem
     )
     own.start()
     own.wait()
+    load.wait()
+    span = att.shape[1]
+    projected = jnp.zeros(base_ref.shape, jnp.float32)
+    for d in range(n_tp):
+        if d:
+            att_copy(d).wait_recv()
+        source = (t - d + n_tp) % n_tp
+        projected = projected + jnp.dot(
+            gathered[source],
+            weight[pl.ds(pl.multiple_of(source * span, span), span), :],
+            preferred_element_type=jnp.float32,
+        )
+    updated = (base_ref[...].astype(jnp.float32) + projected).astype(jnp.bfloat16)
+    updated_ref[...] = updated
+    widened = updated.astype(jnp.float32)
+    mean = jnp.mean(widened * widened, axis=1, keepdims=True)
+    normed_ref[...] = (widened * lax.rsqrt(mean + 1e-06) * norm_ref[...]).astype(jnp.bfloat16)
     for d in range(1, n_tp):
-        att_copy(d).wait()
+        att_copy(d).wait_send()
     for d in range(1, n_z):
         meta_copy(d).wait()
     for d in range(1, n_sp):
@@ -168,8 +194,9 @@
                 kv_copy(d, h).wait_send()
 
 
-def attend(queries, key_pairs, head_values, lambdas, head_gain, meta, rows, n_sp, n_tp):
+def attend(queries, key_pairs, head_values, lambdas, head_gain, meta, residual, norm_gain, out_weight, n_sp, n_tp):
     tokens, heads, pair = queries.shape
+    rows = residual.shape[0]
     width = head_values.shape[2]
     half = pair // 2
     tile = math.gcd(tokens, 256)
@@ -185,12 +212,16 @@
     return pl.pallas_call(
         functools.partial(attend_kernel, n_sp, n_tp, half ** (-0.5)),
         out_shape=(
-            jax.ShapeDtypeStruct((n_tp, rows, heads * width), jnp.bfloat16),
+            jax.ShapeDtypeStruct(residual.shape, jnp.bfloat16),
+            jax.ShapeDtypeStruct(residual.shape, jnp.bfloat16),
             jax.ShapeDtypeStruct((n_z,) + meta.shape, meta.dtype),
         ),
-        in_specs=[pl.BlockSpec(memory_space=pltpu.SMEM)] + [vmem] * 4,
-        out_specs=(vmem, vmem),
+        in_specs=[pl.BlockSpec(memory_space=pltpu.SMEM)] + [vmem] * 6
+        + [pl.BlockSpec(memory_space=pl.ANY)],
+        out_specs=(vmem, vmem, vmem),
         scratch_shapes=[
+            pltpu.VMEM(out_weight.shape, out_weight.dtype),
+            pltpu.VMEM((n_tp, rows, heads * width), jnp.bfloat16),
             pltpu.VMEM((n_sp - 1,) + kv.shape, kv.dtype),
             pltpu.VMEM((heads, tiles, 2 * tile, width), jnp.float32),
             pltpu.VMEM((heads, tiles, 2 * tile, 1), jnp.float32),
@@ -203,12 +234,13 @@
             dma((n_z,)),
             dma((n_z,)),
             dma,
+            dma,
         ],
         compiler_params=pltpu.CompilerParams(
             collective_id=0, has_side_effects=True, vmem_limit_bytes=48 * 1024 * 1024
         ),
         name="attend",
-    )(lambdas, q, kv, head_gain.reshape(1, -1), meta)
+    )(lambdas, q, kv, head_gain.reshape(1, -1), meta, residual, norm_gain.reshape(1, -1), out_weight)
 
 
 def experts_kernel(
@@ -233,6 +265,7 @@
     ret,
     zsend,
     zret,
+    mine,
     w_sem,
     zs_send,
     zs_recv,
@@ -291,19 +324,21 @@
 
     def pack_copy(d, s):
         return remote(
-            pack.at[d - 1, s], arrived.at[0, d, s], ps_send.at[d, s], ps_recv.at[d, s], column(d)
+            pack.at[s, d - 1], arrived.at[0, s, d], ps_send.at[d, s], ps_recv.at[d, s], column(d)
         )
 
     def share_copy(d, s):
         return remote(
-            arrived.at[0, d, s], arrived.at[1, d, s], fw_send.at[d, s], fw_recv.at[d, s], partner
-        )
-
-    def pair_copy(d):
-        return remote(psend.at[d], precv.at[d], pp_send.at[d], pp_recv.at[d], partner)
-
-    def back_copy(d):
-        return remote(own.at[d], ret.at[d], rt_send.at[d], rt_recv.at[d], column(n_sp - d))
+            arrived.at[0, s, d], arrived.at[1, s, d], fw_send.at[d, s], fw_recv.at[d, s], partner
+        )
+
+    def pair_copy(s):
+        return remote(psend.at[s], precv.at[s], pp_send.at[s], pp_recv.at[s], partner)
+
+    def back_copy(d, s):
+        return remote(
+            own.at[s, d], ret.at[s, d], rt_send.at[d, s], rt_recv.at[d, s], column(n_sp - d)
+        )
 
     def z_back(d):
         return remote(
@@ -317,7 +352,7 @@
         target = lax.broadcasted_iota(jnp.int32, (slots, rows), 0).astype(jnp.float32)
         return target == meta_ref[s, r : r + 1, :rows]
 
-    for s in range(n_z):
+    def pack_rows(s):
         if s:
             z_copy(s).wait_recv()
         hits = route_hits(s, 0) | route_hits(s, 1)
@@ -329,58 +364,52 @@
             .reshape(n_sp, local, cap, model)
         )
         for d in range(1, n_sp):
-            pack[d - 1, s] = packed[d]
+            pack[s, d - 1] = packed[d]
             pack_copy(d, s).start()
-        arrived[0, 0, s] = packed[0]
+        arrived[0, s, 0] = packed[0]
         share_copy(0, s).start()
 
-    for load in loads:
-        load.wait()
-
-    def reduce_pair(d):
-        pair_copy(d).wait_recv()
-        total = own[d].astype(jnp.float32) + precv[d].astype(jnp.float32)
-        total = total.astype(jnp.bfloat16)
-        if d == 0:
-            ret[0] = total
-        else:
-            own[d] = total
-            back_copy(d).start()
-
-    for d in range(n_sp):
-        if d:
-            for s in range(n_z):
-                pack_copy(d, s).wait_recv()
-                share_copy(d, s).start()
-        for s in range(n_z):
+    def run_experts(s):
+        for d in range(1, n_sp):
+            pack_copy(d, s).wait_recv()
+            share_copy(d, s).start()
+        for d in range(n_sp):
             share_copy(d, s).wait_recv()
 
         def expert_step(e, carry):
-            x = arrived[:, d, :, e].reshape(2 * n_z * cap, model)
+            x = arrived[:, s, :, e].reshape(2 * n_sp * cap, model)
             gated = jnp.dot(x, gate[e], preferred_element_type=jnp.float32)
             lifted = jnp.dot(x, up[e], preferred_element_type=jnp.float32)
             inner = (gated / (1.0 + jnp.exp(-gated)) * lifted).astype(jnp.bfloat16)
             y = jnp.dot(inner, down[e], preferred_element_type=jnp.float32)
-            y = y.astype(jnp.bfloat16).reshape(2, n_z, cap, model)
-            own[d, :, e] = y[0]
-            psend[d, :, e] = y[1]
+            y = y.astype(jnp.bfloat16).reshape(2, n_sp, cap, model)
+            own[s, :, e] = y[0]
+            psend[s, :, e] = y[1]
             return carry
 
         lax.fori_loop(0, local, expert_step, 0)
-        pair_copy(d).start()
-        if d:
-            reduce_pair(d - 1)
-    reduce_pair(n_sp - 1)
-    for d in range(1, n_sp):
-        back_copy(d).wait_recv()
-
-    for s in list(range(1, n_z)) + [0]:
+        pair_copy(s).start()
+
+    def reduce_pair(s):
+        pair_copy(s).wait_recv()
+        for d in list(range(1, n_sp)) + [0]:
+            total = own[s, d].astype(jnp.float32) + precv[s, d].astype(jnp.float32)
+            total = total.astype(jnp.bfloat16)
+            if d == 0:
+                ret[s, 0] = total
+            else:
+                own[s, d] = total
+                back_copy(d, s).start()
+
+    def mix_rows(s):
+        for d in range(1, n_sp):
+            back_copy(d, s).wait_recv()
         mixing = jnp.where(route_hits(s, 0), meta_ref[s, 2:3, :rows], 0.0) + jnp.where(
             route_hits(s, 1), meta_ref[s, 3:4, :rows], 0.0
         )
         high = mixing.astype(jnp.bfloat16)
         low = (mixing - high.astype(jnp.float32)).astype(jnp.bfloat16)
-        back = ret[:, s].reshape(slots, model)
+        back = ret[s].reshape(slots, model)
         numbers = (((0,), (0,)), ((), ()))
         merged = lax.dot_general(
             high, back, numbers, preferred_element_type=jnp.float32
@@ -388,6 +417,24 @@
         if s:
             zsend[s] = merged.astype(jnp.bfloat16)
             z_back(s).start()
+        else:
+            mine[...] = merged
+
+    pack_rows(0)
+    for load in loads:
+        load.wait()
+    if n_z > 1:
+        pack_rows(1)
+    for s in range(n_z):
+        run_experts(s)
+        if s + 2 < n_z:
+            pack_rows(s + 2)
+        elif s + 2 - n_z < n_z - 2:
+            mix_rows(s + 2 - n_z)
+        reduce_pair(s)
+    for s in range(max(0, n_z - 2), n_z):
+        mix_rows(s)
+    merged = mine[...]
     for s in range(1, n_z):
         z_back(s).wait_recv()
         merged = merged + zret[s].astype(jnp.float32)
@@ -396,14 +443,13 @@
     for d in range(1, n_z):
         z_copy(d).wait_send()
         z_back(d).wait_send()
-    for d in range(n_sp):
-        for s in range(n_z):
+    for s in range(n_z):
+        for d in range(n_sp):
             if d:
                 pack_copy(d, s).wait_send()
+                back_copy(d, s).wait_send()
             share_copy(d, s).wait_send()
-        pair_copy(d).wait_send()
-        if d:
-            back_copy(d).wait_send()
+        pair_copy(s).wait_send()
 
 
 def experts(normed, zmeta, updated, gate_weight, up_weight, down_weight, n_sp, n_z, cap):
@@ -412,7 +458,7 @@
     dma = pltpu.SemaphoreType.DMA
     vmem = pl.BlockSpec(memory_space=pltpu.VMEM)
     hbm = pl.BlockSpec(memory_space=pl.ANY)
-    block = (n_z, local, cap, model)
+    block = (local, cap, model)
 
     def buffer(*shape):
         return pltpu.VMEM(shape, jnp.bfloat16)
@@ -427,14 +473,15 @@
             buffer(*up_weight.shape),
             buffer(*down_weight.shape),
             buffer(n_z - 1, rows, model),
-            buffer(n_sp - 1, *block),
-            buffer(2, n_sp, *block),
-            buffer(n_sp, *block),
-            buffer(n_sp, *block),
-            buffer(n_sp, *block),
-            buffer(n_sp, *block),
+            buffer(n_z, n_sp - 1, *block),
+            buffer(2, n_z, n_sp, *block),
+            buffer(n_z, n_sp, *block),
+            buffer(n_z, n_sp, *block),
+            buffer(n_z, n_sp, *block),
+            buffer(n_z, n_sp, *block),
             buffer(n_z, rows, model),
             buffer(n_z, rows, model),
+            pltpu.VMEM((rows, model), jnp.float32),
             dma((3,)),
             dma((n_z,)),
             dma((n_z,)),
@@ -442,10 +489,10 @@
             dma((n_sp, n_z)),
             dma((n_sp, n_z)),
             dma((n_sp, n_z)),
-            dma((n_sp,)),
-            dma((n_sp,)),
-            dma((n_sp,)),
-            dma((n_sp,)),
+            dma((n_z,)),
+            dma((n_z,)),
+            dma((n_sp, n_z)),
+            dma((n_sp, n_z)),
             dma((n_z,)),
             dma((n_z,)),
         ],
@@ -491,16 +538,19 @@
     slots = flat_ids * capacity + ranking
     meta = jnp.concatenate([near_slots.astype(jnp.float32), route_weights], axis=1).T
     meta = jnp.pad(meta, ((0, 8 - 2 * route_count), (0, -rows_here % 128)), constant_values=-1.0)
-    gathered, zmeta = attend(
-        queries, key_pairs, head_values, lambdas, head_gain, meta, rows_here, sp_count, tp_count
-    )
-    regrouped = jnp.transpose(gathered, (1, 0, 2)).reshape(rows_here, -1)
-    projected = jnp.dot(regrouped, out_weight, preferred_element_type=jnp.float32)
-    updated = (residual.astype(jnp.float32) + projected).astype(jnp.bfloat16)
-    widened = updated.astype(jnp.float32)
-    normed = (
-        widened * lax.rsqrt(jnp.mean(widened * widened, axis=1, keepdims=True) + 1e-06) * norm_gain
-    ).astype(jnp.bfloat16)
+    updated, normed, zmeta = attend(
+        queries,
+        key_pairs,
+        head_values,
+        lambdas,
+        head_gain,
+        meta,
+        residual,
+        norm_gain,
+        out_weight,
+        sp_count,
+        tp_count,
+    )
     model_width = normed.shape[1]
     block_bytes = z_count * local_experts * capacity * model_width * 2
     if capacity % 16 == 0 and rows_here <= 128 and route_count == 2 and (

time: 228 us -> 192 us (0.84)
  Pallas kernels: 212 us -> 182 us
  matrix products: 5.01 us -> 0 us
    pallas_call x1, Pallas kernels: 171 us -> 141 us  [experts(): pl.pallas_call(functools.partial(experts_kernel, n_sp, n_z), out_shape=ja...]
    dot_general x1 -> x0, matrix products: 5.01 us -> none  [shards(): jnp.dot(regrouped, out_weight, preferred_element_type=jnp.float32)]
    unnamed x12 -> x20, local copies, waits for them, and re-layouts: 4.58 us -> 5.37 us
where the time goes in v2:
time: 192 us; the launch traced here: 191 us
  Pallas kernels  182 us (95%)
  local copies, waits for them, and re-layouts  7.11 us (4%)
  other arithmetic  2.3 us (1%)
    pallas_call x1, Pallas kernels, experts(): pl.pallas_call(functools.partial(experts_kernel, n_sp, n_z), out_shape=ja...  141 us
    pallas_call x1, Pallas kernels, attend(): pl.pallas_call(functools.partial(attend_kernel, n_sp, n_tp, half ** (-0.5...  40.3 us
    unnamed x20, local copies, waits for them, and re-layouts  5.37 us

profile of v2, /device:TPU:0, one launch (start us, length us, event | category | flops | bytes accessed | tf_op | source)
XLA Modules:
  0.0 191.1 jit_solution(5723656514383899226)
XLA Ops:
  0.0 0.0 copy-start.7
  0.0 0.0 copy-start.8
  0.0 0.8 copy.20
  0.9 0.1 eq.24
  1.0 0.6 reduce-window.6
  1.6 0.2 slice_reduce_fusion
  1.9 0.1 add_bitcast_fusion
  2.0 0.1 sub.16
  2.1 0.1 copy.21
  2.2 0.7 fusion.4
  2.9 0.7 maximum_bitcast_fusion.1
  3.6 1.1 copy.17
  4.7 0.0 copy-start
  4.7 0.0 copy-start.4
  4.7 0.0 copy-start.5
  4.7 0.0 copy-start.6
  4.7 0.1 bitcast_select_fusion.q_ref
  4.8 0.0 copy-done.7
  4.8 0.0 copy-done.8
  4.8 0.1 copy_bitcast_fusion
  4.9 0.1 maximum_bitcast_fusion.kv_ref
  5.0 0.7 copy-done
  5.7 0.0 copy-done.4
  5.7 0.0 copy-done.5
  5.7 0.0 copy-done.6
  5.7 40.3 %attend.1 = (bf16[96,2048]{1,0:T(8,128)(2,1)S(1)}, bf16[96,2048]{1,0:T(8,128)(2,1)S(1)}, f32[4,8,128]{2,1,0:T(8,128)S(1)}) custom-call(f32[2]{0:T(128)S(1)} %copy-done.5, bf16[2,3,512,128]{3,2,1,0:T(8,128)(2,1)S(1)} %bitcast_select_fusion.q_ref, bf16[2,2,768,128]{3,2,1,0:T(8,128)(2,1)S(1)} %maximum_bitcast_fusion.kv_ref, f32[1,128]{1,0:T(1,128)S(1)} %bitcast.25, ...), custom_call_target="tpu_custom_call" | custom-call | tf_op jit(solution)/shard_map/attend/pallas_call | solution.py:212
  46.0 0.0 copy-start.1
  46.0 0.7 copy-done.1
  46.7 0.0 copy-start.2
  46.7 0.7 copy-done.2
  47.5 0.0 copy-start.3
  47.5 0.6 copy-done.3
  48.1 141.3 %experts.1 = bf16[96,2048]{1,0:T(8,128)(2,1)} custom-call(bf16[96,2048]{1,0:T(8,128)(2,1)} %copy-done.2, f32[4,8,128]{2,1,0:T(8,128)} %copy-done.3, bf16[96,2048]{1,0:T(8,128)(2,1)} %copy-done.1, bf16[2,2048,256]{2,1,0:T(8,128)(2,1)} %gate_hbm.1, bf16[2,2048,256]{2,1,0:T(8,128)(2,1)} %up_hbm.1, bf16[2,256,2048]{2,1,0:T(8,128)(2,1)} %down_hbm.1), custom_call_target="tpu_custom_call" | custom-call | tf_op jit(solution)/shard_map/experts/pallas_call | solution.py:466
  189.4 1.8 copy.25
  (10 shorter events, 0.1 us)
Async XLA Ops:
  0.0 4.8 %copy-start.7 = (bf16[768,2,128]{2,1,0:T(2,128)(2,1)S(1)}, bf16[768,2,128]{2,1,0:T(2,128)(2,1)}, u32[]{:S(2)}) copy-start(bf16[768,2,128]{2,1,0:T(2,128)(2,1)} %param.15) | copy-start | bytes 1179652
  0.0 4.8 %copy-start.8 = (bf16[768,2,128]{2,1,0:T(2,128)(2,1)S(1)}, bf16[768,2,128]{2,1,0:T(2,128)(2,1)}, u32[]{:S(2)}) copy-start(bf16[768,2,128]{2,1,0:T(2,128)(2,1)} %param.14) | copy-start | bytes 1179652
  4.7 1.0 copy-start
  4.7 1.0 copy-start.4
  4.7 1.0 copy-start.5
  4.7 1.0 copy-start.6
  46.0 0.7 copy-start.1
  46.7 0.7 copy-start.2
  47.5 0.6 copy-start.3
